TPU v7x, 32 devices: a whole 2x2x4 slice. The times are simulated.
32 devices in a mesh: ep: 8 (over z, x), tp: 4 (over y, core).
Axes of the slice: x: 2, y: 2, z: 4, core: 2. Of those that a mesh axis runs over, the one named last changes fastest.
Arguments:
- queries: bfloat16 [2048, 8, 128], P('ep', 'tp'), may hold values from -256 to 256
- keys: bfloat16 [2048, 4, 128], P('ep', 'tp'), may hold values from -8 to 8
- values: bfloat16 [2048, 4, 128], P('ep', 'tp'), may hold values from -6 to 6
- attn_lambda: float32 [8], P('tp'), may hold values from 0.3 to 0.8
- head_gain: float32 [128], replicated, may hold values from 0.1 to 1.9
- w_out: bfloat16 [1024, 2048], replicated, may hold values from -0.1875 to 0.1875
- moe_rows: bfloat16 [4096, 2048], P('ep'), may hold values from -6 to 6
- moe_gain: float32 [2048], replicated, may hold values from 0.1 to 1.9
- routes: int32 [4096, 2], P('ep'), may hold values from 0 to 7, all different within a row; in each aligned block of 128 rows (0 to 127, 128 to 255, ...) at most 64 rows name the same one
- route_weights: float32 [4096, 2], P('ep'), may hold values from 0.1 to 1
- w_gate: bfloat16 [8, 2048, 1024], P('ep', None, 'tp'), may hold values from -0.125 to 0.125
- w_up: bfloat16 [8, 2048, 1024], P('ep', None, 'tp'), may hold values from -0.125 to 0.125
- w_down: bfloat16 [8, 1024, 2048], P('ep', 'tp'), may hold values from -0.1875 to 0.1875
Outputs:
- mixer_out: bfloat16 [2048, 2048], P(('ep', 'tp'))
- moe_out: bfloat16 [4096, 2048], P(('ep', 'tp'))
Inputs may be any that keep to these rules, and one draw needn't show every extreme that they name: `routes`: each row names 2 different experts. In each aligned block of 128 rows (the rows of moe_out that one device holds) no expert is named by more than 64 rows, a bound that some block reaches.
All inputs are finite; a program needn't handle non-finite values.
Results may differ from a plain program's by a relative error of at most 0.011.
Values may be sent and summed in bfloat16 or wider, within the bound.
A program may use at most 128 MiB of HBM per device.

v0:
```python
import jax
import jax.numpy as jnp
from jax import lax
from jax.sharding import PartitionSpec as P

EPSILON = 1e-06
MASKED = -1e30


def rms_scaled(values_f, gain):
    mean_sq = jnp.mean(values_f * values_f, axis=-1, keepdims=True)
    return values_f * lax.rsqrt(mean_sq + EPSILON) * gain


def slot_numbers(block_routes, experts):
    flat_ids = block_routes.reshape(-1)
    matches = (flat_ids[:, None] == lax.iota(jnp.int32, experts)[None, :]).astype(jnp.int32)
    earlier = jnp.cumsum(matches, axis=0) - matches
    return jnp.sum(earlier * matches, axis=1).reshape(block_routes.shape)


def fill_slots(block_rows, block_routes, experts, capacity):
    slot_ids = slot_numbers(block_routes, experts)
    model_width = block_rows.shape[1]
    copies = jnp.broadcast_to(block_rows[:, None, :], block_routes.shape + (model_width,))
    blank_slots = jnp.zeros((experts, capacity, model_width), block_rows.dtype)
    return (blank_slots.at[block_routes, slot_ids].set(copies), slot_ids)


def local(
    queries,
    keys,
    values,
    attn_lambda,
    head_gain,
    w_out,
    moe_rows,
    moe_gain,
    routes,
    route_weights,
    w_gate,
    w_up,
    w_down,
):
    positions = queries.shape[0]
    q_heads = queries.shape[1]
    kv_heads = keys.shape[1]
    head_dim = queries.shape[2] // 2
    value_dim = values.shape[2]
    per_key = q_heads // kv_heads
    first_pos = lax.axis_index("ep") * positions
    query_pos = first_pos + lax.iota(jnp.int32, positions)
    last_pos = first_pos + positions - 1
    query_view = queries.reshape(positions, kv_heads, per_key, 2, head_dim)
    inv_scale = head_dim ** (-0.5)
    start_max = jnp.full((positions, kv_heads, per_key, 2), MASKED, jnp.float32)
    start_total = jnp.zeros((positions, kv_heads, per_key, 2), jnp.float32)
    start_acc = jnp.zeros((positions, kv_heads, per_key, 2, value_dim), jnp.float32)
    carry = (start_max, start_total, start_acc)
    key_piece = lax.all_gather(keys, "ep", axis=0, tiled=True)
    value_piece = lax.all_gather(values, "ep", axis=0, tiled=True)
    shard_count = key_piece.shape[0] // positions
    together = 1
    for candidate in (2, 3, 4):
        if shard_count % candidate == 0:
            together = candidate
    block_len = together * positions
    blocks = shard_count // together
    key_blocks = key_piece.reshape(blocks, block_len, kv_heads, 2, head_dim)
    value_blocks = value_piece.reshape(blocks, block_len, kv_heads, value_dim)
    block_starts = block_len * lax.iota(jnp.int32, blocks)

    def visit(running, inputs):
        key_blk, value_blk, block_start = inputs

        def update(current):
            run_max, run_total, run_acc = current
            key_pos = block_start + lax.iota(jnp.int32, block_len)
            scores = (
                jnp.einsum(
                    "qkgmd,pkmd->qkgmp", query_view, key_blk, preferred_element_type=jnp.float32
                )
                * inv_scale
            )
            allowed = key_pos[None, :] <= query_pos[:, None]
            scores = jnp.where(allowed[:, None, None, None, :], scores, MASKED)
            new_max = jnp.maximum(run_max, jnp.max(scores, axis=-1))
            shrink = jnp.exp(run_max - new_max)
            weights = jnp.exp(scores - new_max[..., None])
            run_total = run_total * shrink + jnp.sum(weights, axis=-1)
            run_acc = run_acc * shrink[..., None] + jnp.einsum(
                "qkgmp,pkv->qkgmv",
                weights.astype(jnp.bfloat16),
                value_blk,
                preferred_element_type=jnp.float32,
            )
            return (new_max, run_total, run_acc)

        def keep(current):
            return current

        return (lax.cond(block_start <= last_pos, update, keep, running), None)

    carry, unused = lax.scan(visit, carry, (key_blocks, value_blocks, block_starts))
    run_max, run_total, run_acc = carry
    ratios = run_acc / run_total[..., None]
    lambda_view = attn_lambda.reshape(1, kv_heads, per_key, 1)
    head_out = ratios[:, :, :, 0] - lambda_view * ratios[:, :, :, 1]
    attn_rows = (
        rms_scaled(head_out, head_gain).astype(jnp.bfloat16).reshape(positions, q_heads * value_dim)
    )
    tp_count = lax.axis_size("tp")
    tp_id = lax.axis_index("tp")
    exchanged = lax.all_to_all(
        attn_rows.reshape(positions, q_heads, value_dim),
        "tp",
        split_axis=0,
        concat_axis=1,
        tiled=True,
    )
    mixer_out = jnp.dot(
        exchanged.reshape(positions // tp_count, tp_count * q_heads * value_dim),
        w_out,
        preferred_element_type=jnp.float32,
    ).astype(jnp.bfloat16)
    experts = lax.axis_size("ep")
    dev_rows = moe_rows.shape[0] // tp_count
    top_count = routes.shape[1]
    capacity = max(2, 2 * dev_rows * top_count // experts)
    model_width = moe_rows.shape[1]
    hidden_units = w_gate.shape[2]
    own_routes = lax.dynamic_slice_in_dim(routes, tp_id * dev_rows, dev_rows, 0)
    own_weights = lax.dynamic_slice_in_dim(route_weights, tp_id * dev_rows, dev_rows, 0)
    own_rows = rms_scaled(
        lax.dynamic_slice_in_dim(moe_rows, tp_id * dev_rows, dev_rows, 0).astype(jnp.float32),
        moe_gain,
    ).astype(jnp.bfloat16)
    outgoing, own_slots = fill_slots(own_rows, own_routes, experts, capacity)
    arrived = lax.all_to_all(outgoing, "ep", split_axis=0, concat_axis=0, tiled=True)
    slot_rows = lax.all_gather(arrived[None], "tp", axis=0, tiled=True)
    flat_rows = slot_rows.reshape(-1, model_width)
    gate_out = jnp.dot(flat_rows, w_gate[0], preferred_element_type=jnp.float32)
    up_out = jnp.dot(flat_rows, w_up[0], preferred_element_type=jnp.float32)
    hidden = (
        (jax.nn.silu(gate_out) * up_out)
        .astype(jnp.bfloat16)
        .reshape(slot_rows.shape[:-1] + (hidden_units,))
    )
    flat_terms = hidden.reshape(-1, hidden_units)
    summed = lax.psum_scatter(
        jnp.dot(flat_terms, w_down[0], preferred_element_type=jnp.float32)
        .reshape(hidden.shape[:-1] + (model_width,))
        .astype(jnp.bfloat16),
        "tp",
        scatter_dimension=0,
        tiled=True,
    )
    returned = lax.all_to_all(summed, "ep", split_axis=1, concat_axis=1, tiled=True)[0]
    picked = returned[own_routes, own_slots]
    moe_out = jnp.sum(own_weights[..., None] * picked.astype(jnp.float32), axis=1).astype(
        jnp.bfloat16
    )
    return (mixer_out, moe_out)


def solution(mesh):
    return jax.shard_map(
        local,
        mesh=mesh,
        in_specs=(
            P("ep", "tp", None),
            P("ep", "tp", None),
            P("ep", "tp", None),
            P("tp"),
            P(),
            P(),
            P("ep", None),
            P(),
            P("ep", None),
            P("ep", None),
            P("ep", None, "tp"),
            P("ep", None, "tp"),
            P("ep", "tp", None),
        ),
        out_specs=(P(("ep", "tp"), None), P(("ep", "tp"), None)),
        check_vma=False,
    )
```

profile of v0, /device:TPU:0, one launch (start us, length us, event | category | flops | bytes accessed | tf_op | source)
XLA Modules:
  0.0 330.0 jit_solution(4695768976303798606)
XLA Ops:
  7.2 0.8 constant_dynamic-slice_fusion
  8.4 0.6 reduce-window.6
  9.7 1.2 fusion.24
  10.9 1.3 fusion.26
  12.2 0.6 broadcast_in_dim.60
  12.8 1.2 reshape.233
  14.3 33.4 %scatter_fusion = bf16[8,64,2048]{2,1,0:T(8,128)(2,1)S(1)} fusion(bf16[8,64,2048]{2,1,0:T(8,128)(2,1)S(1)} %broadcast_in_dim.58, s32[256]{0:T(256)S(1)} %reshape.231, bf16[256,2048]{1,0:T(8,128)(2,1)} %reshape.233), kind=kCustom, calls=%fused_computation.1 | custom fusion | bytes 3147776 | tf_op jit(solution)/shard_map/scatter | solution.py:27
  47.7 55.4 %all_to_all.25 = bf16[8,64,2048]{2,1,0:T(8,128)(2,1)} all-to-all(bf16[8,64,2048]{2,1,0:T(8,128)(2,1)S(1)} %scatter_fusion), channel_id=1, replica_groups=mesh['ep'=8,'tp'=4] {'ep'}, dimensions={0} | all-to-all | bytes 4194304 | tf_op jit(solution)/shard_map/all_to_all | solution.py:139
  103.2 57.4 %all-gather.3.cloned.1.call-done = bf16[32,64,2048]{2,1,0:T(8,128)(2,1)} async-done(((bf16[8,64,2048]{2,1,0:T(8,128)(2,1)}), bf16[32,64,2048]{2,1,0:T(8,128)(2,1)}) %all-gather.3.cloned.1.call-update) | async-done | bytes 8388624 | tf_op jit(solution)/shard_map/all_gather | solution.py:140
  160.6 5.9 %fusion.29 = f32[2048,256]{1,0:T(8,128)S(1)} fusion(bf16[2048,2048]{1,0:T(8,128)(2,1)} %bitcast.134, bf16[1,2048,256]{2,1,0:T(8,128)(2,1)S(1)} %copy-done.7), kind=kOutput, calls=%fused_computation.40 | convolution fusion | flops 2147483648 | bytes 11534336 | tf_op jit(solution)/shard_map/dot_general | solution.py:142
  166.6 2.6 fusion.23
  169.2 5.6 %convolution_convert_fusion = bf16[4,8,64,2048]{3,2,1,0:T(8,128)(2,1)} fusion(bf16[4,8,64,256]{3,2,1,0:T(8,128)(2,1)S(1)} %bitcast.130, bf16[1,256,2048]{2,1,0:T(8,128)(2,1)S(1)} %copy-done), kind=kOutput, calls=%fused_computation.28 | convolution fusion | flops 2151677952 | bytes 10485760 | tf_op jit(solution)/shard_map/dot_general | solution.py:151
  174.8 0.8 copy-done.2
  175.6 31.4 %all_gather.9 = bf16[2048,1,128]{2,0,1:T(8,128)(2,1)S(1)} all-gather(bf16[256,1,128]{2,0,1:T(8,128)(2,1)S(1)} %copy-done.2), channel_id=1, replica_groups=mesh['ep'=8,'tp'=4] {'ep'}, dimensions={0}, use_global_device_ids=true | all-gather | bytes 589824 | tf_op jit(solution)/shard_map/all_gather | solution.py:60
  207.5 0.7 copy.64
  208.3 31.4 %all_gather.10 = bf16[2048,1,128]{2,0,1:T(8,128)(2,1)S(1)} all-gather(bf16[256,1,128]{2,0,1:T(8,128)(2,1)S(1)} %copy-done.3), channel_id=1, replica_groups=mesh['ep'=8,'tp'=4] {'ep'}, dimensions={0}, use_global_device_ids=true | all-gather | bytes 589824 | tf_op jit(solution)/shard_map/all_gather | solution.py:61
  240.1 5.6 %while.15 = (s32[]{:T(128)}, f32[256,1,2,2]{0,2,3,1:T(2,128)S(1)}, f32[256,1,2,2]{0,2,3,1:T(2,128)S(1)}, f32[256,1,2,2,128]{0,4,3,2,1:T(8,128)S(1)}, s32[2]{0:T(...) while((s32[]{:T(128)}, f32[256,1,2,2]{0,2,3,1:T(2,128)S(1)}, ...), condition=%wide.region_5.6_spmd.clone, body=%wide.region_0.5_spmd.clone.sunk | while | flops 411570432 | bytes 15155487 | solution.py:104
  240.2 0.6 dynamic_slice.50
  241.3 3.3 conditional.3
  241.3 0.6 iota_add_fusion
  242.1 0.9 fusion.4
  243.0 1.0 fusion.5
  244.6 0.6 dynamic_slice.50
  246.1 0.7 broadcast_divide_fusion
  247.8 7.0 %all_to_all.26 = bf16[256,2,128]{2,1,0:T(2,128)(2,1)S(1)} all-to-all(bf16[256,2,128]{2,1,0:T(2,128)(2,1)S(1)} %fusion.37), channel_id=1, replica_groups=mesh['ep'=8,'tp'=4] {'tp'}, dimensions={0} | all-to-all | bytes 262144 | tf_op jit(solution)/shard_map/all_to_all | solution.py:114
  254.8 8.9 %all-to-all-start.2 = ((bf16[1,8,64,2048]{3,2,0,1:T(8,128)(2,1)}), bf16[1,8,64,2048]{3,2,0,1:T(8,128)(2,1)S(1)}, u32[]{:S(2)}, u32[]{:S(2)}) async-start(bf16[1,8,64,2048]{3,2,0,1:T(8,128)(2,1)} %bitcast.127), calls=%async_computation.3 | async-start | bytes 4194304 | tf_op jit(solution)/shard_map/all_to_all | solution.py:158
  263.9 0.7 constant_dynamic-slice_fusion.1
  264.9 3.7 %convolution_convert_fusion.1 = bf16[64,2048]{1,0:T(8,128)(2,1)} fusion(bf16[64,1024]{1,0:T(8,128)(2,1)S(1)} %reshape.221, bf16[1024,2048]{1,0:T(8,128)(2,1)} %param.22), kind=kOutput, calls=%fused_computation.31 | convolution fusion | flops 268566528 | bytes 4587520 | tf_op jit(solution)/shard_map/dot_general | solution.py:121
  268.6 42.9 %all-to-all-done.2 = bf16[1,8,64,2048]{3,2,0,1:T(8,128)(2,1)S(1)} async-done(((bf16[1,8,64,2048]{3,2,0,1:T(8,128)(2,1)}), bf16[1,8,64,2048]{3,2,0,1:T(8,128)(2,1)S(1)}, u32[]{:S(2)}, u32[]{:S(2)}) %all-to-all-start.2) | async-done | bytes 2097184 | tf_op jit(solution)/shard_map/all_to_all | solution.py:158
  311.6 5.3 %gather_fusion = bf16[256,2048]{1,0:T(8,128)(2,1)} fusion(bf16[8,64,2048]{2,1,0:T(8,128)(2,1)S(1)} %bitcast.126, s32[256]{0:T(256)S(1)} %reshape.225), kind=kCustom, calls=%fused_computation | custom fusion | bytes 2099200 | tf_op jit(solution)/shard_map/gather | solution.py:159
  316.9 2.4 reshape.239
  319.3 3.9 %multiply_reduce_fusion = bf16[128,2048]{1,0:T(8,128)(2,1)} fusion(f32[128,2,2048]{2,1,0:T(2,128)S(1)} %reshape.239, f32[128,2]{1,0:T(8,128)S(1)} %copy.73), kind=kLoop, calls=%fused_computation.32 | loop fusion | flops 786432 | bytes 2622464 | tf_op jit(solution)/shard_map/reduce_sum | solution.py:160
  (63 shorter events, 4.9 us)
Async XLA Ops:
  7.2 162.1 %copy-start = (bf16[1,256,2048]{2,1,0:T(8,128)(2,1)S(1)}, bf16[1,256,2048]{2,1,0:T(8,128)(2,1)}, u32[]{:S(2)}) copy-start(bf16[1,256,2048]{2,1,0:T(8,128)(2,1)} %param.29) | copy-start | bytes 3145732
  7.2 153.4 %all-gather.3.cloned.1.call-start = ((), (), s32[]{:S(2)}) async-start(), calls=%async_computation.5 | async-start | bytes 10485760 | tf_op jit(solution)/shard_map/all_gather | solution.py:140
  103.1 57.5 %copy-start.7 = (bf16[1,2048,256]{2,1,0:T(8,128)(2,1)S(1)}, bf16[1,2048,256]{2,1,0:T(8,128)(2,1)}, u32[]{:S(2)}) copy-start(bf16[1,2048,256]{2,1,0:T(8,128)(2,1)} %param.27) | copy-start | bytes 3145732
  103.1 151.7 %reduce-scatter.2.cloned.1.call-start = ((), (), s32[]{:S(2)}) async-start(), calls=%async_computation.4 | async-start | bytes 10485760 | tf_op jit(solution)/shard_map/reduce_scatter | solution.py:150
  160.6 5.9 %copy-start.6 = (bf16[32,64,2048]{2,1,0:T(8,128)(2,1)S(1)}, bf16[32,64,2048]{2,1,0:T(8,128)(2,1)}, u32[]{:S(2)}) copy-start(bf16[32,64,2048]{2,1,0:T(8,128)(2,1)} %all-gather.3.cloned.1.call-done) | copy-start | bytes 25165828
  160.6 6.0 %copy-start.8 = (bf16[1,2048,256]{2,1,0:T(8,128)(2,1)S(1)}, bf16[1,2048,256]{2,1,0:T(8,128)(2,1)}, u32[]{:S(2)}) copy-start(bf16[1,2048,256]{2,1,0:T(8,128)(2,1)} %param.28) | copy-start | bytes 3145732
  174.8 0.8 copy-start.2
  174.8 33.4 %copy-start.3 = (bf16[256,1,128]{2,0,1:T(8,128)(2,1)S(1)}, bf16[256,1,128]{2,0,1:T(8,128)(2,1)}, u32[]{:S(2)}) copy-start(bf16[256,1,128]{2,0,1:T(8,128)(2,1)} %param.19) | copy-start | bytes 196612
  207.1 32.8 %copy-start.1 = (bf16[256,2,128]{2,1,0:T(2,128)(2,1)S(1)}, bf16[256,2,128]{2,1,0:T(2,128)(2,1)}, u32[]{:S(2)}) copy-start(bf16[256,2,128]{2,1,0:T(2,128)(2,1)} %param.17) | copy-start | bytes 393220
  245.7 1.1 copy-start.4
  245.7 1.6 copy-start.5
  254.8 56.8 %all-to-all-start.2 = ((bf16[1,8,64,2048]{3,2,0,1:T(8,128)(2,1)}), bf16[1,8,64,2048]{3,2,0,1:T(8,128)(2,1)S(1)}, u32[]{:S(2)}, u32[]{:S(2)}) async-start(bf16[1,8,64,2048]{3,2,0,1:T(8,128)(2,1)} %bitcast.127), calls=%async_computation.3 | async-start | bytes 4194304 | tf_op jit(solution)/shard_map/all_to_all | solution.py:158
Sparse Core Ops, SparseCore 0:
  103.2 57.2 all-gather.2
  174.9 71.3 reduce-scatter.1
where the time goes:
time: 331 us; the launch traced here: 330 us
  blocking collectives  125 us (38%)
  waiting for transfers between devices  100 us (30%)
  local copies, waits for them, and re-layouts  49.9 us (15%)
  matrix products  19.2 us (6%)
  between operations  14.4 us (4%)
  other arithmetic  10.6 us (3%)
  starting transfers between devices  9.02 us (3%)
    all_gather x1, waiting for transfers between devices, local(): slot_rows = lax.all_gather(arrived[None], 'tp', axis=0, tiled=True)  57.4 us
    all_to_all x1, blocking collectives, local(): lax.all_to_all(outgoing, 'ep', split_axis=0, concat_axis=0, tiled=True)  55.4 us
    all_to_all x1, waiting for transfers between devices, local(): lax.all_to_all(summed, 'ep', split_axis=1, concat_axis=1, tiled=True)[0]  42.9 us
    scatter x1, local copies, waits for them, and re-layouts, fill_slots(): return (blank_slots.at[block_routes, slot_ids].set(copies), slot_ids)  33.4 us
    all_gather x1, blocking collectives, local(): key_piece = lax.all_gather(keys, 'ep', axis=0, tiled=True)  31.4 us
    all_gather x1, blocking collectives, local(): value_piece = lax.all_gather(values, 'ep', axis=0, tiled=True)  31.4 us
    all_to_all x1, starting transfers between devices, local(): lax.all_to_all(summed, 'ep', split_axis=1, concat_axis=1, tiled=True)[0]  8.94 us
    all_to_all x1, blocking collectives, local(): lax.all_to_all(attn_rows.reshape(positions, q_heads, value_dim), 'tp', sp...  6.99 us
  transfers between devices with their start and end apart: 3, of which 2 were waited for; matrix products, arithmetic and copies ran while one was open for 4% of the time, Pallas kernels for 0%

commit v1 on v0

--- a/solution.py
+++ b/solution.py
@@ -1,3 +1,4 @@
+import functools
 import jax
 import jax.numpy as jnp
 from jax import lax
@@ -5,6 +6,24 @@
 
 EPSILON = 1e-06
 MASKED = -1e30
+
+
+def page_rest(a0, shard_axis, axis_k):
+    dev_n = jax.lax.axis_size(shard_axis)
+    sides = []
+    for w in range(dev_n):
+        sides.append((w, (w + 1) % dev_n))
+    r2 = [None] * dev_n
+    r2[dev_n - 1] = a0
+    for c in range(dev_n - 2, -1, -1):
+        r2[c] = jax.lax.ppermute(r2[c + 1], shard_axis, sides)
+    wide_out = jnp.concatenate(r2, axis_k)
+    near = (jax.lax.axis_index(shard_axis) + 1) * a0.shape[axis_k]
+    lower = jnp.roll(wide_out, near, axis_k)
+    return lower
+
+
+_obtain_view = functools.partial(page_rest, shard_axis="tp", axis_k=0)
 
 
 def rms_scaled(values_f, gain):
@@ -137,7 +156,7 @@
     ).astype(jnp.bfloat16)
     outgoing, own_slots = fill_slots(own_rows, own_routes, experts, capacity)
     arrived = lax.all_to_all(outgoing, "ep", split_axis=0, concat_axis=0, tiled=True)
-    slot_rows = lax.all_gather(arrived[None], "tp", axis=0, tiled=True)
+    slot_rows = _obtain_view(arrived[None])
     flat_rows = slot_rows.reshape(-1, model_width)
     gate_out = jnp.dot(flat_rows, w_gate[0], preferred_element_type=jnp.float32)
     up_out = jnp.dot(flat_rows, w_up[0], preferred_element_type=jnp.float32)

time: 331 us -> 378 us (1.14)
  local copies, waits for them, and re-layouts: 49.9 us -> 78.3 us
  waiting for transfers between devices: 100 us -> 120 us
    ppermute x0 -> x3, waiting for transfers between devices: none -> 76.8 us  [page_rest(): r2[c] = jax.lax.ppermute(r2[c + 1], shard_axis, sides)]
    all_gather x1 -> x0, waiting for transfers between devices: 57.4 us -> none  [local(): slot_rows = lax.all_gather(arrived[None], 'tp', axis=0, tiled=True)]
    unnamed x23 -> x36, local copies, waits for them, and re-layouts: 2.13 us -> 20.7 us
    dynamic_slice x0 -> x1, local copies, waits for them, and re-layouts: none -> 8.35 us  [page_rest(): lower = jnp.roll(wide_out, near, axis_k)]
  transfers between devices with their start and end apart: 3 -> 5, of which waited for: 2 -> 4; matrix products, arithmetic and copies ran while one was open for 4% -> 3% of each run, Pallas kernels for 0% -> 0%
where the time goes in v1:
time: 378 us; the launch traced here: 376 us
  blocking collectives  126 us (33%)
  waiting for transfers between devices  120 us (32%)
  local copies, waits for them, and re-layouts  78.3 us (21%)
  matrix products  19.5 us (5%)
  between operations  14.4 us (4%)
  other arithmetic  10.6 us (3%)
  starting transfers between devices  6.73 us (2%)
    ppermute x3, waiting for transfers between devices, page_rest(): r2[c] = jax.lax.ppermute(r2[c + 1], shard_axis, sides)  76.8 us
    all_to_all x1, blocking collectives, local(): lax.all_to_all(outgoing, 'ep', split_axis=0, concat_axis=0, tiled=True)  55.3 us
    all_to_all x1, waiting for transfers between devices, local(): lax.all_to_all(summed, 'ep', split_axis=1, concat_axis=1, tiled=True)[0]  43 us
    scatter x1, local copies, waits for them, and re-layouts, fill_slots(): return (blank_slots.at[block_routes, slot_ids].set(copies), slot_ids)  33.4 us
    all_gather x1, blocking collectives, local(): value_piece = lax.all_gather(values, 'ep', axis=0, tiled=True)  31.6 us
    all_gather x1, blocking collectives, local(): key_piece = lax.all_gather(keys, 'ep', axis=0, tiled=True)  31.2 us
    unnamed x36, local copies, waits for them, and re-layouts  20.7 us
    dynamic_slice x1, local copies, waits for them, and re-layouts, page_rest(): lower = jnp.roll(wide_out, near, axis_k)  8.35 us
  transfers between devices with their start and end apart: 5, of which 4 were waited for; matrix products, arithmetic and copies ran while one was open for 3% of the time, Pallas kernels for 0%

profile of v1, /device:TPU:0, one launch (start us, length us, event | category | flops | bytes accessed | tf_op | source)
XLA Modules:
  0.0 376.3 jit_solution(12243224926325539768)
XLA Ops:
  9.7 1.2 fusion.24
  10.9 1.3 fusion.26
  12.8 1.2 reshape.233
  14.3 33.4 %scatter_fusion = bf16[8,64,2048]{2,1,0:T(8,128)(2,1)S(1)} fusion(bf16[8,64,2048]{2,1,0:T(8,128)(2,1)S(1)} %broadcast_in_dim.58, s32[256]{0:T(256)S(1)} %reshape.231, bf16[256,2048]{1,0:T(8,128)(2,1)} %reshape.233), kind=kCustom, calls=%fused_computation.1 | custom fusion | bytes 3147776 | tf_op jit(solution)/shard_map/scatter | solution.py:46
  47.7 55.3 %all_to_all.25 = bf16[8,64,2048]{2,1,0:T(8,128)(2,1)S(1)} all-to-all(bf16[8,64,2048]{2,1,0:T(8,128)(2,1)S(1)} %scatter_fusion), channel_id=1, replica_groups=mesh['ep'=8,'tp'=4] {'ep'}, dimensions={0} | all-to-all | bytes 4194304 | tf_op jit(solution)/shard_map/all_to_all | solution.py:158
  103.0 1.3 copy-done.2
  104.3 25.5 %collective-permute-done = bf16[1,8,64,2048]{3,2,1,0:T(8,128)(2,1)S(1)} collective-permute-done((bf16[1,8,64,2048]{3,2,1,0:T(8,128)(2,1)S(1)}, bf16[1,8,64,2048]{3,2,1,0:T(8,128)(2,1)S(1)}, u32[]{:S(2)}, u32[]{:S(2)}) %collective-permute-start) | collective-permute-done | bytes 2097184 | tf_op jit(solution)/shard_map/ppermute | solution.py:19
  129.8 25.6 %collective-permute-done.1 = bf16[1,8,64,2048]{3,2,1,0:T(8,128)(2,1)} collective-permute-done((bf16[1,8,64,2048]{3,2,1,0:T(8,128)(2,1)S(1)}, bf16[1,8,64,2048]{3,2,1,0:T(8,128)(2,1)}, u32[]{:S(2)}, u32[]{:S(2)}) %collective-permute-start.1) | collective-permute-done | bytes 2097184 | tf_op jit(solution)/shard_map/ppermute | solution.py:19
  155.3 25.8 %collective-permute-done.2 = bf16[1,8,64,2048]{3,2,1,0:T(8,128)(2,1)} collective-permute-done((bf16[1,8,64,2048]{3,2,1,0:T(8,128)(2,1)}, bf16[1,8,64,2048]{3,2,1,0:T(8,128)(2,1)}, u32[]{:S(2)}, u32[]{:S(2)}) %collective-permute-start.2) | collective-permute-done | bytes 2097184 | tf_op jit(solution)/shard_map/ppermute | solution.py:19
  181.1 3.2 constant_dynamic-update-slice_fusion.7
  184.3 3.3 constant_dynamic-update-slice_fusion.6
  187.6 1.5 constant_dynamic-update-slice_fusion.5
  189.1 1.5 constant_dynamic-update-slice_fusion.4
  190.5 3.2 constant_dynamic-update-slice_fusion.3
  193.8 3.1 constant_dynamic-update-slice_fusion.2
  196.9 1.5 constant_dynamic-update-slice_fusion.1
  198.4 1.5 constant_dynamic-update-slice_fusion
  199.9 8.4 %constant_dynamic-slice_fusion = bf16[4,8,64,2048]{3,2,1,0:T(8,128)(2,1)} fusion(bf16[8,8,64,2048]{3,2,1,0:T(8,128)(2,1)} %constant_dynamic-update-slice_fusion, s32[]{:T(128)S(6)} %select_n.43), kind=kLoop, calls=%fused_computation.78 | loop fusion | bytes 16777220 | tf_op jit(solution)/shard_map/jit(_roll_dynamic)/dynamic_slice | solution.py:22
  208.2 6.0 %fusion.29 = f32[2048,256]{1,0:T(8,128)S(1)} fusion(bf16[2048,2048]{1,0:T(8,128)(2,1)} %bitcast.131, bf16[1,2048,256]{2,1,0:T(8,128)(2,1)S(1)} %copy-done.10), kind=kOutput, calls=%fused_computation.40 | convolution fusion | flops 2147483648 | bytes 11534336 | tf_op jit(solution)/shard_map/dot_general | solution.py:161
  214.3 2.8 fusion.23
  217.0 5.6 %convolution_convert_fusion = bf16[4,8,64,2048]{3,2,1,0:T(8,128)(2,1)} fusion(bf16[4,8,64,256]{3,2,1,0:T(8,128)(2,1)S(1)} %bitcast.136, bf16[1,256,2048]{2,1,0:T(8,128)(2,1)S(1)} %copy-done), kind=kOutput, calls=%fused_computation.28 | convolution fusion | flops 2151677952 | bytes 10485760 | tf_op jit(solution)/shard_map/dot_general | solution.py:170
  223.5 31.2 %all_gather.6 = bf16[2048,1,128]{2,0,1:T(8,128)(2,1)S(1)} all-gather(bf16[256,1,128]{2,0,1:T(8,128)(2,1)S(1)} %copy-done.6), channel_id=1, replica_groups=mesh['ep'=8,'tp'=4] {'ep'}, dimensions={0}, use_global_device_ids=true | all-gather | bytes 589824 | tf_op jit(solution)/shard_map/all_gather | solution.py:79
  255.9 31.6 %all_gather.7 = bf16[2048,1,128]{2,0,1:T(8,128)(2,1)S(1)} all-gather(bf16[256,1,128]{2,0,1:T(8,128)(2,1)S(1)} %copy-done.7), channel_id=1, replica_groups=mesh['ep'=8,'tp'=4] {'ep'}, dimensions={0}, use_global_device_ids=true | all-gather | bytes 589824 | tf_op jit(solution)/shard_map/all_gather | solution.py:80
  288.0 5.6 %while.15 = (s32[]{:T(128)}, f32[256,1,2,2]{0,2,3,1:T(2,128)S(1)}, f32[256,1,2,2]{0,2,3,1:T(2,128)S(1)}, f32[256,1,2,2,128]{0,4,3,2,1:T(8,128)S(1)}, s32[2]{0:T(...) while((s32[]{:T(128)}, f32[256,1,2,2]{0,2,3,1:T(2,128)S(1)}, ...), condition=%wide.region_5.6_spmd.clone, body=%wide.region_0.5_spmd.clone.sunk | while | flops 411570432 | bytes 15155487 | solution.py:123
  289.1 3.3 conditional.3
  295.6 7.6 %all_to_all.26 = bf16[256,2,128]{2,1,0:T(2,128)(2,1)S(1)} all-to-all(bf16[256,2,128]{2,1,0:T(2,128)(2,1)S(1)} %fusion.37), channel_id=1, replica_groups=mesh['ep'=8,'tp'=4] {'tp'}, dimensions={0} | all-to-all | bytes 262144 | tf_op jit(solution)/shard_map/all_to_all | solution.py:133
  303.2 6.7 %all-to-all-start.2 = ((bf16[1,8,64,2048]{3,2,0,1:T(8,128)(2,1)}), bf16[1,8,64,2048]{3,2,0,1:T(8,128)(2,1)S(1)}, u32[]{:S(2)}, u32[]{:S(2)}) async-start(bf16[1,8,64,2048]{3,2,0,1:T(8,128)(2,1)} %bitcast.133), calls=%async_computation.3 | async-start | bytes 4194304 | tf_op jit(solution)/shard_map/all_to_all | solution.py:177
  311.1 3.7 convolution_convert_fusion.1
  314.8 43.0 %all-to-all-done.2 = bf16[1,8,64,2048]{3,2,0,1:T(8,128)(2,1)S(1)} async-done(((bf16[1,8,64,2048]{3,2,0,1:T(8,128)(2,1)}), bf16[1,8,64,2048]{3,2,0,1:T(8,128)(2,1)S(1)}, u32[]{:S(2)}, u32[]{:S(2)}) %all-to-all-start.2) | async-done | bytes 2097184 | tf_op jit(solution)/shard_map/all_to_all | solution.py:177
  357.8 5.3 %gather_fusion = bf16[256,2048]{1,0:T(8,128)(2,1)} fusion(bf16[8,64,2048]{2,1,0:T(8,128)(2,1)S(1)} %bitcast.129, s32[256]{0:T(256)S(1)} %reshape.225), kind=kCustom, calls=%fused_computation | custom fusion | bytes 2099200 | tf_op jit(solution)/shard_map/gather | solution.py:178
  363.1 2.4 reshape.237
  365.5 3.9 %multiply_reduce_fusion = bf16[128,2048]{1,0:T(8,128)(2,1)} fusion(f32[128,2,2048]{2,1,0:T(2,128)S(1)} %reshape.237, f32[128,2]{1,0:T(8,128)S(1)} %copy.73), kind=kLoop, calls=%fused_computation.32 | loop fusion | flops 786432 | bytes 2622464 | tf_op jit(solution)/shard_map/reduce_sum | solution.py:179
  (81 shorter events, 13.2 us)
Async XLA Ops:
  7.2 209.9 %copy-start = (bf16[1,256,2048]{2,1,0:T(8,128)(2,1)S(1)}, bf16[1,256,2048]{2,1,0:T(8,128)(2,1)}, u32[]{:S(2)}) copy-start(bf16[1,256,2048]{2,1,0:T(8,128)(2,1)} %param.29) | copy-start | bytes 3145732
  7.2 296.1 %reduce-scatter.2.cloned.1.call-start = ((), (), s32[]{:S(2)}) async-start(), calls=%async_computation.4 | async-start | bytes 10485760 | tf_op jit(solution)/shard_map/reduce_scatter | solution.py:169
  103.0 1.3 copy-start.2
  104.3 25.5 %collective-permute-start = (bf16[1,8,64,2048]{3,2,1,0:T(8,128)(2,1)S(1)}, bf16[1,8,64,2048]{3,2,1,0:T(8,128)(2,1)S(1)}, u32[]{:S(2)}, u32[]{:S(2)}) collective-permute-start(bf16[1,8,64,2048]{3,2,1,0:T(8,128)(2,1)S(1)} %bitcast.130), channel_id=1, source_target_pairs={{0,1},{1,2},{2,3},{3,0},{4,5},{5,6},{6,7},{7,4},{8,9},{9,10},{10,1... | collective-permute-start | bytes 6291464 | tf_op jit(solution)/shard_map/ppermute | solution.py:19
  129.8 25.6 %collective-permute-start.1 = (bf16[1,8,64,2048]{3,2,1,0:T(8,128)(2,1)S(1)}, bf16[1,8,64,2048]{3,2,1,0:T(8,128)(2,1)}, u32[]{:S(2)}, u32[]{:S(2)}) collective-permute-start(bf16[1,8,64,2048]{3,2,1,0:T(8,128)(2,1)S(1)} %collective-permute-done), channel_id=1, source_target_pairs={{0,1},{1,2},{2,3},{3,0},{4,5},{5,6},{6,7},{7,4},{8,9},{9,10},{10,1... | collective-permute-start | bytes 6291464 | tf_op jit(solution)/shard_map/ppermute | solution.py:19
  155.3 25.8 %collective-permute-start.2 = (bf16[1,8,64,2048]{3,2,1,0:T(8,128)(2,1)}, bf16[1,8,64,2048]{3,2,1,0:T(8,128)(2,1)}, u32[]{:S(2)}, u32[]{:S(2)}) collective-permute-start(bf16[1,8,64,2048]{3,2,1,0:T(8,128)(2,1)} %collective-permute-done.1), channel_id=1, source_target_pairs={{0,1},{1,2},{2,3},{3,0},{4,5},{5,6},{6,7},{7,4},{8,9},{9,10},{10,1... | collective-permute-start | bytes 6291464 | tf_op jit(solution)/shard_map/ppermute | solution.py:19
  184.3 4.8 %copy-start.3 = (bf16[8,64,2048]{2,1,0:T(8,128)(2,1)S(1)}, bf16[8,64,2048]{2,1,0:T(8,128)(2,1)}, u32[]{:S(2)}) copy-start(bf16[8,64,2048]{2,1,0:T(8,128)(2,1)} %copy-done.2) | copy-start | bytes 6291460
  199.9 8.4 %copy-start.10 = (bf16[1,2048,256]{2,1,0:T(8,128)(2,1)S(1)}, bf16[1,2048,256]{2,1,0:T(8,128)(2,1)}, u32[]{:S(2)}) copy-start(bf16[1,2048,256]{2,1,0:T(8,128)(2,1)} %param.27) | copy-start | bytes 3145732
  208.2 6.0 %copy-start.4 = (bf16[4,8,64,2048]{3,2,1,0:T(8,128)(2,1)S(1)}, bf16[4,8,64,2048]{3,2,1,0:T(8,128)(2,1)}, u32[]{:S(2)}) copy-start(bf16[4,8,64,2048]{3,2,1,0:T(8,128)(2,1)} %constant_dynamic-slice_fusion) | copy-start | bytes 25165828
  208.2 6.0 %copy-start.11 = (bf16[1,2048,256]{2,1,0:T(8,128)(2,1)S(1)}, bf16[1,2048,256]{2,1,0:T(8,128)(2,1)}, u32[]{:S(2)}) copy-start(bf16[1,2048,256]{2,1,0:T(8,128)(2,1)} %param.28) | copy-start | bytes 3145732
  222.6 0.8 copy-start.6
  222.6 33.3 %copy-start.7 = (bf16[256,1,128]{2,0,1:T(8,128)(2,1)S(1)}, bf16[256,1,128]{2,0,1:T(8,128)(2,1)}, u32[]{:S(2)}) copy-start(bf16[256,1,128]{2,0,1:T(8,128)(2,1)} %param.19) | copy-start | bytes 196612
  222.6 65.1 %copy-start.5 = (bf16[256,2,128]{2,1,0:T(2,128)(2,1)S(1)}, bf16[256,2,128]{2,1,0:T(2,128)(2,1)}, u32[]{:S(2)}) copy-start(bf16[256,2,128]{2,1,0:T(2,128)(2,1)} %param.17) | copy-start | bytes 393220
  288.0 6.7 %copy-start.8 = (f32[2]{0:T(128)S(1)}, f32[2]{0:T(128)}, u32[]{:S(2)}) copy-start(f32[2]{0:T(128)} %param.20) | copy-start | bytes 28
  288.0 7.2 %copy-start.9 = (f32[128]{0:T(128)S(1)}, f32[128]{0:T(128)}, u32[]{:S(2)}) copy-start(f32[128]{0:T(128)} %param.21) | copy-start | bytes 1540
  303.2 54.6 %all-to-all-start.2 = ((bf16[1,8,64,2048]{3,2,0,1:T(8,128)(2,1)}), bf16[1,8,64,2048]{3,2,0,1:T(8,128)(2,1)S(1)}, u32[]{:S(2)}, u32[]{:S(2)}) async-start(bf16[1,8,64,2048]{3,2,0,1:T(8,128)(2,1)} %bitcast.133), calls=%async_computation.3 | async-start | bytes 4194304 | tf_op jit(solution)/shard_map/all_to_all | solution.py:177
  357.8 11.6 %copy-start.1 = (bf16[1,256,2048]{2,1,0:T(8,128)(2,1)S(1)}, bf16[1,256,2048]{2,1,0:T(8,128)(2,1)}, u32[]{:S(2)}) copy-start(bf16[1,256,2048]{2,1,0:T(8,128)(2,1)} %param.29) | copy-start | bytes 3145732
Sparse Core Ops, SparseCore 0:
  222.8 70.4 reduce-scatter.1
